TPU v7x, 32 devices: a whole 2x2x4 slice. The times are simulated.
32 devices in a mesh: sp: 8 (over z, x), tp: 4 (over y, core).
Axes of the slice: x: 2, y: 2, z: 4, core: 2. Of those that a mesh axis runs over, the one named last changes fastest.
Arguments:
- cotangent: bfloat16 [1024, 2048], P('sp'), may hold values from -6 to 6
- mixer_out: bfloat16 [1024, 2048], P('sp'), may hold values from -6 to 6
- expert_ids: int32 [1024, 2], P('sp'), may hold values from 0 to 7, all different within a row; in each aligned block of 128 rows (0 to 127, 128 to 255, ...) at most 64 rows name the same one
- route_weight: float32 [1024, 2], P('sp'), may hold values from 0.3 to 1.5
- saved_normalized: bfloat16 [1024, 2048], P('sp', 'tp'), may hold values from -6 to 6
- inverse_deviation: float32 [1024], P('sp'), may hold values from 0.3 to 3
- channel_norm_gain: float32 [2048], P('tp'), may hold values from 0.1 to 1.9
- taps: float32 [31, 2048], P(None, 'tp'), may hold values from -1 to 1
- proj_weight: bfloat16 [2048, 2048], P('tp'), may hold values from -0.125 to 0.125
- gate_weight: bfloat16 [8, 2048, 2048], P('sp', None, 'tp'), may hold values from -0.125 to 0.125
- up_weight: bfloat16 [8, 2048, 2048], P('sp', None, 'tp'), may hold values from -0.125 to 0.125
- down_weight: bfloat16 [8, 2048, 2048], P('sp', 'tp'), may hold values from -0.125 to 0.125
Outputs:
- grad_mixer_in: bfloat16 [1024, 2048], P('sp', 'tp')
- grad_proj: float32 [2048, 2048], P('sp', 'tp')
- grad_gate: bfloat16 [8, 2048, 2048], P('sp', None, 'tp')
- grad_up: bfloat16 [8, 2048, 2048], P('sp', None, 'tp')
- grad_down: bfloat16 [8, 2048, 2048], P('sp', 'tp')
Inputs may be any that keep to these rules, and one draw needn't show every extreme that they name: `expert_ids`: each row names 2 different experts. Within the rows of one index of sp no expert is named more than 64 times, a bound that some block reaches.
All inputs are finite; a program needn't handle non-finite values.
Results may differ from a plain program's by a relative error of at most 0.02.
Values may be sent and summed in bfloat16 or wider, within the bound.
A program may use at most 64 MiB of HBM per device.

v0:
```python
import jax
import jax.numpy as jnp
from jax import lax
from jax.sharding import PartitionSpec as P


def from_behind(value, axis, steps):
    count = lax.axis_size(axis)
    leading, last = (max(0, -steps), min(count, count - steps))
    return lax.ppermute(value, axis, [(source, source + steps) for source in range(leading, last)])


def route_table(expert_ids, route_weight, slot_start, slot_span, capacity, experts):
    onehot = (expert_ids[:, :, None] == jnp.arange(experts, dtype=jnp.int32)[None, None, :]).astype(
        jnp.int32
    )
    flat_hot = onehot.reshape(-1, experts)
    ranks = jnp.cumsum(flat_hot, axis=0) - flat_hot
    rank_pair = jnp.sum(ranks * flat_hot, axis=1).reshape(expert_ids.shape)
    slot_index = expert_ids * capacity + rank_pair
    targets = (
        jnp.arange(experts, dtype=jnp.int32)[:, None] * capacity
        + slot_start
        + jnp.arange(slot_span, dtype=jnp.int32)[None, :]
    ).reshape(-1)
    matched = slot_index[None, :, :] == targets[:, None, None]
    dispatch = jnp.any(matched, axis=2).astype(jnp.bfloat16)
    slot_weight = jnp.sum(jnp.where(matched, route_weight[None, :, :], 0.0), axis=(1, 2))
    return (dispatch, slot_weight)


def shards(
    cotangent,
    mixer_out,
    expert_ids,
    route_weight,
    saved_normalized,
    inverse_deviation,
    channel_norm_gain,
    taps,
    proj_weight,
    gate_weight,
    up_weight,
    down_weight,
):
    experts = lax.axis_size("sp")
    groups = lax.axis_size("tp")
    tok_rows, model_width = cotangent.shape
    capacity = groups * max(1, 4 * tok_rows // (experts * groups))
    slot_span = capacity // groups
    slot_start = lax.axis_index("tp") * slot_span
    dispatch, slot_weight = route_table(
        expert_ids, route_weight, slot_start, slot_span, capacity, experts
    )
    sent_rows = jnp.dot(dispatch, mixer_out, preferred_element_type=jnp.float32).astype(
        jnp.bfloat16
    )
    sent_grad = (
        slot_weight[:, None] * jnp.dot(dispatch, cotangent, preferred_element_type=jnp.float32)
    ).astype(jnp.bfloat16)
    sent_rows = sent_rows.reshape(experts, slot_span, model_width)
    sent_grad = sent_grad.reshape(experts, slot_span, model_width)
    shared_rows = (
        lax.all_to_all(sent_rows, "sp", split_axis=0, concat_axis=0, tiled=True),
        lax.all_to_all(sent_grad, "sp", split_axis=0, concat_axis=0, tiled=True),
    )
    routed_rows, routed_grad = (
        lax.all_gather(shared_rows[0], "tp", axis=1, tiled=True),
        lax.all_gather(shared_rows[1], "tp", axis=1, tiled=True),
    )
    full_table, unused_weight = route_table(
        expert_ids, route_weight, 0, capacity, capacity, experts
    )
    routed_rows = routed_rows.reshape(-1, model_width)
    routed_grad = routed_grad.reshape(-1, model_width)
    w_first = gate_weight[0]
    w_third = up_weight[0]
    w_second = down_weight[0]
    contract_last = (((1,), (1,)), ((), ()))
    contract_first = (((0,), (0,)), ((), ()))
    hidden_gate = jnp.dot(routed_rows, w_first, preferred_element_type=jnp.float32)
    hidden_up = jnp.dot(routed_rows, w_third, preferred_element_type=jnp.float32)
    sigma = jax.nn.sigmoid(hidden_gate)
    swish = hidden_gate * sigma
    activ = (swish * hidden_up).astype(jnp.bfloat16)
    grad_second = lax.dot_general(
        activ, routed_grad, contract_first, preferred_element_type=jnp.float32
    ).astype(jnp.bfloat16)
    grad_activ = lax.dot_general(
        routed_grad, w_second, contract_last, preferred_element_type=jnp.float32
    )
    grad_gpre = (grad_activ * hidden_up * sigma * (1.0 + hidden_gate * (1.0 - sigma))).astype(
        jnp.bfloat16
    )
    grad_upre = (grad_activ * swish).astype(jnp.bfloat16)
    grad_first = lax.dot_general(
        routed_rows, grad_gpre, contract_first, preferred_element_type=jnp.float32
    ).astype(jnp.bfloat16)
    grad_third = lax.dot_general(
        routed_rows, grad_upre, contract_first, preferred_element_type=jnp.float32
    ).astype(jnp.bfloat16)
    partial_value = lax.dot_general(
        grad_gpre, w_first, contract_last, preferred_element_type=jnp.float32
    ) + lax.dot_general(grad_upre, w_third, contract_last, preferred_element_type=jnp.float32)
    summed = lax.psum(partial_value.astype(jnp.bfloat16), "tp")
    home_rows = lax.all_to_all(
        summed.reshape(experts, capacity, model_width),
        "sp",
        split_axis=0,
        concat_axis=0,
        tiled=True,
    )
    returned = lax.dot_general(
        full_table,
        home_rows.reshape(-1, model_width),
        contract_first,
        preferred_element_type=jnp.float32,
    )
    mixer_grad = (cotangent.astype(jnp.float32) + returned).astype(jnp.bfloat16)
    normalized_input = saved_normalized.astype(jnp.float32)
    normalized_values = normalized_input * channel_norm_gain[None, :]
    gate_sig = jax.nn.sigmoid(normalized_values)
    act_conv = (normalized_values * gate_sig).astype(jnp.bfloat16)
    grad_proj = lax.psum_scatter(
        lax.dot_general(
            mixer_grad, act_conv, contract_first, preferred_element_type=jnp.float32
        ).astype(jnp.bfloat16),
        "sp",
        scatter_dimension=0,
        tiled=True,
    ).astype(jnp.float32)
    grad_act = lax.dot_general(
        mixer_grad, proj_weight, contract_last, preferred_element_type=jnp.float32
    )
    norm_output_gradient = (
        grad_act
        * gate_sig
        * (1.0 + normalized_values * (1.0 - gate_sig))
        * channel_norm_gain[None, :]
    )
    reduced_totals = lax.psum(
        (
            jnp.sum(norm_output_gradient, axis=1),
            jnp.sum(norm_output_gradient * normalized_input, axis=1),
        ),
        "tp",
    )
    channel_count = saved_normalized.shape[1] * groups
    conv_output_gradient = inverse_deviation[:, None] * (
        norm_output_gradient
        - reduced_totals[0][:, None] / channel_count
        - normalized_input * (reduced_totals[1][:, None] / channel_count)
    )
    reach = taps.shape[0] - 1
    beyond = from_behind(conv_output_gradient[:reach], "sp", -1)
    extended = jnp.concatenate([conv_output_gradient, beyond], axis=0)
    result = jnp.zeros_like(conv_output_gradient)
    for tap_index in range(taps.shape[0]):
        result = result + taps[tap_index][None, :] * extended[tap_index : tap_index + tok_rows]
    return (
        result.astype(jnp.bfloat16),
        grad_proj,
        grad_first[None],
        grad_third[None],
        grad_second[None],
    )


def solution(mesh):
    return jax.shard_map(
        shards,
        mesh=mesh,
        in_specs=(
            P("sp", None),
            P("sp", None),
            P("sp", None),
            P("sp", None),
            P("sp", "tp"),
            P("sp"),
            P("tp"),
            P(None, "tp"),
            P("tp", None),
            P("sp", None, "tp"),
            P("sp", None, "tp"),
            P("sp", "tp", None),
        ),
        out_specs=(
            P("sp", "tp"),
            P("sp", "tp"),
            P("sp", None, "tp"),
            P("sp", None, "tp"),
            P("sp", "tp", None),
        ),
        check_vma=False,
    )
```

profile of v0, /device:TPU:0, one launch (start us, length us, event | category | flops | bytes accessed | tf_op | source)
XLA Modules:
  0.0 273.1 jit_solution(8081440627756328696)
XLA Ops:
  7.3 0.9 copy.31
  8.6 0.6 reduce-window.6
  9.8 0.7 multiply_add_fusion
  10.6 1.3 convolution_convert_fusion.4
  11.9 21.7 %all_to_all.15 = bf16[8,16,2048]{2,1,0:T(8,128)(2,1)} all-to-all(bf16[8,16,2048]{2,1,0:T(8,128)(2,1)S(1)} %bitcast.87), channel_id=1, replica_groups=mesh['sp'=8,'tp'=4] {'sp'}, dimensions={0} | all-to-all | bytes 1048576 | tf_op jit(solution)/shard_map/all_to_all | solution.py:64
  34.2 17.6 %all_to_all.16 = bf16[8,16,2048]{2,1,0:T(8,128)(2,1)} all-to-all(bf16[8,16,2048]{2,1,0:T(8,128)(2,1)S(1)} %bitcast.86), channel_id=1, replica_groups=mesh['sp'=8,'tp'=4] {'sp'}, dimensions={0} | all-to-all | bytes 1048576 | tf_op jit(solution)/shard_map/all_to_all | solution.py:65
  51.9 3.5 %all-gather.5.cloned.1.call-done = bf16[8,64,2048]{2,1,0:T(8,128)(2,1)} async-done(((bf16[8,16,2048]{2,1,0:T(8,128)(2,1)}), bf16[8,64,2048]{2,1,0:T(8,128)(2,1)}) %all-gather.5.cloned.1.call-update) | async-done | bytes 2097168 | tf_op jit(solution)/shard_map/all_gather | solution.py:68
  55.4 4.0 %fusion.7 = f32[512,512]{1,0:T(8,128)} fusion(bf16[512,2048]{1,0:T(8,128)(2,1)} %bitcast.119, bf16[1,2048,512]{2,1,0:T(8,128)(2,1)S(1)} %copy-done), kind=kOutput, calls=%fused_computation.44 | convolution fusion | flops 1073741824 | bytes 5242880 | tf_op jit(solution)/shard_map/dot_general | solution.py:81
  59.4 2.3 fusion.10
  61.7 17.9 %all-gather.3.cloned.1.call-done = bf16[8,64,2048]{2,1,0:T(8,128)(2,1)} async-done(((bf16[8,16,2048]{2,1,0:T(8,128)(2,1)}), bf16[8,64,2048]{2,1,0:T(8,128)(2,1)}) %all-gather.3.cloned.1.call-update) | async-done | bytes 2097168 | tf_op jit(solution)/shard_map/all_gather | solution.py:69
  79.6 4.4 %multiply_convert_fusion.1 = (bf16[512,512]{1,0:T(8,128)(2,1)S(1)}, bf16[512,512]{1,0:T(8,128)(2,1)S(1)}) fusion(f32[512,512]{1,0:T(8,128)} %fusion.7, f32[512,512]{1,0:T(8,128)} %fusion.10, bf16[512,2048]{1,0:T(8,128)(2,1)} %bitcast.123, bf16[1,512,2048]{2,1,0:T(8,128)(2,1)} %param.23), kind=kOutput, calls=%fused_computation.55 | convolution fusion | flops 1077149696 | bytes 7340032 | tf_op jit(solution)/shard_map/dot_general | solution.py:89
  84.0 1.3 fusion.5
  85.3 0.6 copy-done.2
  85.9 2.6 add_convert_fusion
  88.6 51.5 %all-reduce.3.cloned.1.call-done = bf16[8,64,2048]{2,1,0:T(8,128)(2,1)} async-done(((bf16[8,64,2048]{2,1,0:T(8,128)(2,1)}), bf16[8,64,2048]{2,1,0:T(8,128)(2,1)}) %all-reduce.3.cloned.1.call-update) | async-done | bytes 2097168 | tf_op jit(solution)/shard_map/psum | solution.py:105
  140.1 5.5 %all-to-all-start.2 = ((bf16[8,64,2048]{2,1,0:T(8,128)(2,1)}), bf16[8,64,2048]{2,1,0:T(8,128)(2,1)}, u32[]{:S(2)}, u32[]{:S(2)}) async-start(bf16[8,64,2048]{2,1,0:T(8,128)(2,1)} %all-reduce.3.cloned.1.call-done), calls=%async_computation.2 | async-start | bytes 4194304 | tf_op jit(solution)/shard_map/all_to_all | solution.py:106
  146.0 47.7 %all-to-all-done.2 = bf16[8,64,2048]{2,1,0:T(8,128)(2,1)} async-done(((bf16[8,64,2048]{2,1,0:T(8,128)(2,1)}), bf16[8,64,2048]{2,1,0:T(8,128)(2,1)}, u32[]{:S(2)}, u32[]{:S(2)}) %all-to-all-start.2) | async-done | bytes 2097184 | tf_op jit(solution)/shard_map/all_to_all | solution.py:106
  193.7 2.1 fusion.4
  195.8 2.1 convolution_convert_fusion
  198.0 0.6 fusion.130
  198.6 0.7 fusion.129
  199.3 4.4 %fusion.1 = bf16[1,2048,512]{2,1,0:T(8,128)(2,1)} fusion(bf16[512,2048]{1,0:T(8,128)(2,1)} %bitcast.120, bf16[512,512]{1,0:T(8,128)(2,1)S(1)} %copy-done.7), kind=kOutput, calls=%fused_computation.35 | convolution fusion | flops 1074790400 | bytes 4718592 | tf_op jit(solution)/shard_map/dot_general | solution.py:99
  203.7 2.7 fusion.2
  206.4 1.5 fusion.128
  207.9 6.2 %all-reduce = (f32[128]{0:T(128)S(1)}, f32[128]{0:T(128)S(1)}) all-reduce(f32[128]{0:T(128)} %get-tuple-element.6, f32[128]{0:T(128)} %get-tuple-element.5), channel_id=1, replica_groups=mesh['sp'=8,'tp'=4] {'tp'}, use_global_device_ids=true, to_apply=%region_10.11 | all-reduce | flops 256 | bytes 2048 | tf_op jit(solution)/shard_map/psum | solution.py:141
  214.1 0.8 fusion.27
  215.2 1.3 collective-permute-start
  216.5 4.3 %fusion = bf16[1,2048,512]{2,1,0:T(8,128)(2,1)} fusion(bf16[512,2048]{1,0:T(8,128)(2,1)} %bitcast.121, bf16[512,512]{1,0:T(8,128)(2,1)S(1)} %copy-done.5), kind=kOutput, calls=%fused_computation.34 | convolution fusion | flops 1074790400 | bytes 4718592 | tf_op jit(solution)/shard_map/dot_general | solution.py:96
  220.7 0.9 collective-permute-done
  221.9 2.0 fusion.32
  223.9 40.9 %reduce-scatter.2.cloned.1.call-done = bf16[256,512]{1,0:T(8,128)(2,1)} async-done(((bf16[2048,512]{1,0:T(8,128)(2,1)}), bf16[256,512]{1,0:T(8,128)(2,1)}) %reduce-scatter.2.cloned.1.call-update) | async-done | bytes 262160 | tf_op jit(solution)/shard_map/reduce_scatter | solution.py:124
  264.8 1.8 convert_element_type.72
  (118 shorter events, 2.3 us)
Async XLA Ops:
  7.2 48.3 %copy-start = (bf16[1,2048,512]{2,1,0:T(8,128)(2,1)S(1)}, bf16[1,2048,512]{2,1,0:T(8,128)(2,1)}, u32[]{:S(2)}) copy-start(bf16[1,2048,512]{2,1,0:T(8,128)(2,1)} %param.21) | copy-start | bytes 6291460
  7.2 26.5 %copy-start.39 = (f32[128,2]{0,1:T(2,128)S(1)}, f32[128,2]{0,1:T(2,128)}, u32[]{:S(2)}) copy-start(f32[128,2]{0,1:T(2,128)} %param.15) | copy-start | bytes 3076
  7.2 26.7 %copy-start.3 = (bf16[128,2048]{1,0:T(8,128)(2,1)S(1)}, bf16[128,2048]{1,0:T(8,128)(2,1)}, u32[]{:S(2)}) copy-start(bf16[128,2048]{1,0:T(8,128)(2,1)} %param.12) | copy-start | bytes 1572868
  7.2 48.2 %all-gather.5.cloned.1.call-start = ((), (), s32[]{:S(2)}) async-start(), calls=%async_computation.5 | async-start | bytes 2621440 | tf_op jit(solution)/shard_map/all_gather | solution.py:68
  33.7 45.9 %all-gather.3.cloned.1.call-start = ((), (), s32[]{:S(2)}) async-start(), calls=%async_computation.4 | async-start | bytes 2621440 | tf_op jit(solution)/shard_map/all_gather | solution.py:69
  51.9 88.2 %all-reduce.3.cloned.1.call-start = ((), (), s32[]{:S(2)}) async-start(), calls=%async_computation.6 | async-start | bytes 4194304 | tf_op jit(solution)/shard_map/psum | solution.py:105
  140.1 53.6 %all-to-all-start.2 = ((bf16[8,64,2048]{2,1,0:T(8,128)(2,1)}), bf16[8,64,2048]{2,1,0:T(8,128)(2,1)}, u32[]{:S(2)}, u32[]{:S(2)}) async-start(bf16[8,64,2048]{2,1,0:T(8,128)(2,1)} %all-reduce.3.cloned.1.call-done), calls=%async_computation.2 | async-start | bytes 4194304 | tf_op jit(solution)/shard_map/all_to_all | solution.py:106
  145.6 50.2 %copy-start.8 = (bf16[128,512]{1,0:T(8,128)(2,1)S(1)}, bf16[128,512]{1,0:T(8,128)(2,1)}, u32[]{:S(2)}) copy-start(bf16[128,512]{1,0:T(8,128)(2,1)} %param.16) | copy-start | bytes 393220
  145.6 50.2 %copy-start.37 = (f32[512]{0:T(512)S(1)}, f32[512]{0:T(512)}, u32[]{:S(2)}) copy-start(f32[512]{0:T(512)} %param.18) | copy-start | bytes 6148
  145.6 119.1 %reduce-scatter.2.cloned.1.call-start = ((), (), s32[]{:S(2)}) async-start(), calls=%async_computation.7 | async-start | bytes 2359296 | tf_op jit(solution)/shard_map/reduce_scatter | solution.py:124
  206.4 10.0 %copy-start.5 = (bf16[512,512]{1,0:T(8,128)(2,1)S(1)}, bf16[512,512]{1,0:T(8,128)(2,1)}, u32[]{:S(2)}) copy-start(bf16[512,512]{1,0:T(8,128)(2,1)} %copy-done.4) | copy-start | bytes 1572868
  214.9 6.8 %copy-start.10 = (f32[1,512]{1,0:T(1,128)S(1)}, f32[1,512]{1,0:T(1,128)}, u32[]{:S(2)}) copy-start(f32[1,512]{1,0:T(1,128)} %get-tuple-element.34) | copy-start | bytes 6148
  214.9 6.8 %copy-start.11 = (f32[1,512]{1,0:T(1,128)S(1)}, f32[1,512]{1,0:T(1,128)}, u32[]{:S(2)}) copy-start(f32[1,512]{1,0:T(1,128)} %get-tuple-element.35) | copy-start | bytes 6148
  214.9 6.8 %copy-start.12 = (f32[1,512]{1,0:T(1,128)S(1)}, f32[1,512]{1,0:T(1,128)}, u32[]{:S(2)}) copy-start(f32[1,512]{1,0:T(1,128)} %get-tuple-element.36) | copy-start | bytes 6148
  214.9 6.8 %copy-start.13 = (f32[1,512]{1,0:T(1,128)S(1)}, f32[1,512]{1,0:T(1,128)}, u32[]{:S(2)}) copy-start(f32[1,512]{1,0:T(1,128)} %get-tuple-element.37) | copy-start | bytes 6148
  214.9 6.8 %copy-start.14 = (f32[1,512]{1,0:T(1,128)S(1)}, f32[1,512]{1,0:T(1,128)}, u32[]{:S(2)}) copy-start(f32[1,512]{1,0:T(1,128)} %get-tuple-element.38) | copy-start | bytes 6148
  214.9 6.8 %copy-start.15 = (f32[1,512]{1,0:T(1,128)S(1)}, f32[1,512]{1,0:T(1,128)}, u32[]{:S(2)}) copy-start(f32[1,512]{1,0:T(1,128)} %get-tuple-element.39) | copy-start | bytes 6148
  214.9 6.8 %copy-start.16 = (f32[1,512]{1,0:T(1,128)S(1)}, f32[1,512]{1,0:T(1,128)}, u32[]{:S(2)}) copy-start(f32[1,512]{1,0:T(1,128)} %get-tuple-element.40) | copy-start | bytes 6148
  215.0 6.8 %copy-start.17 = (f32[1,512]{1,0:T(1,128)S(1)}, f32[1,512]{1,0:T(1,128)}, u32[]{:S(2)}) copy-start(f32[1,512]{1,0:T(1,128)} %get-tuple-element.41) | copy-start | bytes 6148
  215.0 6.8 %copy-start.18 = (f32[1,512]{1,0:T(1,128)S(1)}, f32[1,512]{1,0:T(1,128)}, u32[]{:S(2)}) copy-start(f32[1,512]{1,0:T(1,128)} %get-tuple-element.11) | copy-start | bytes 6148
  215.0 6.8 %copy-start.19 = (f32[1,512]{1,0:T(1,128)S(1)}, f32[1,512]{1,0:T(1,128)}, u32[]{:S(2)}) copy-start(f32[1,512]{1,0:T(1,128)} %get-tuple-element.12) | copy-start | bytes 6148
  215.0 6.8 %copy-start.20 = (f32[1,512]{1,0:T(1,128)S(1)}, f32[1,512]{1,0:T(1,128)}, u32[]{:S(2)}) copy-start(f32[1,512]{1,0:T(1,128)} %get-tuple-element.13) | copy-start | bytes 6148
  215.0 6.8 %copy-start.21 = (f32[1,512]{1,0:T(1,128)S(1)}, f32[1,512]{1,0:T(1,128)}, u32[]{:S(2)}) copy-start(f32[1,512]{1,0:T(1,128)} %get-tuple-element.14) | copy-start | bytes 6148
  215.0 6.8 %copy-start.22 = (f32[1,512]{1,0:T(1,128)S(1)}, f32[1,512]{1,0:T(1,128)}, u32[]{:S(2)}) copy-start(f32[1,512]{1,0:T(1,128)} %get-tuple-element.15) | copy-start | bytes 6148
  215.0 6.8 %copy-start.23 = (f32[1,512]{1,0:T(1,128)S(1)}, f32[1,512]{1,0:T(1,128)}, u32[]{:S(2)}) copy-start(f32[1,512]{1,0:T(1,128)} %get-tuple-element.16) | copy-start | bytes 6148
  215.0 6.8 %copy-start.24 = (f32[1,512]{1,0:T(1,128)S(1)}, f32[1,512]{1,0:T(1,128)}, u32[]{:S(2)}) copy-start(f32[1,512]{1,0:T(1,128)} %get-tuple-element.17) | copy-start | bytes 6148
  215.0 6.8 %copy-start.25 = (f32[1,512]{1,0:T(1,128)S(1)}, f32[1,512]{1,0:T(1,128)}, u32[]{:S(2)}) copy-start(f32[1,512]{1,0:T(1,128)} %get-tuple-element.18) | copy-start | bytes 6148
  215.0 6.8 %copy-start.26 = (f32[1,512]{1,0:T(1,128)S(1)}, f32[1,512]{1,0:T(1,128)}, u32[]{:S(2)}) copy-start(f32[1,512]{1,0:T(1,128)} %get-tuple-element.19) | copy-start | bytes 6148
  215.1 6.8 %copy-start.27 = (f32[1,512]{1,0:T(1,128)S(1)}, f32[1,512]{1,0:T(1,128)}, u32[]{:S(2)}) copy-start(f32[1,512]{1,0:T(1,128)} %get-tuple-element.20) | copy-start | bytes 6148
  215.1 6.8 %copy-start.28 = (f32[1,512]{1,0:T(1,128)S(1)}, f32[1,512]{1,0:T(1,128)}, u32[]{:S(2)}) copy-start(f32[1,512]{1,0:T(1,128)} %get-tuple-element.21) | copy-start | bytes 6148
  215.1 6.8 %copy-start.29 = (f32[1,512]{1,0:T(1,128)S(1)}, f32[1,512]{1,0:T(1,128)}, u32[]{:S(2)}) copy-start(f32[1,512]{1,0:T(1,128)} %get-tuple-element.22) | copy-start | bytes 6148
  215.2 6.5 %collective-permute-start = (f32[30,512]{1,0:T(8,128)S(1)}, f32[30,512]{1,0:T(8,128)S(1)}, u32[]{:S(2)}, u32[]{:S(2)}) collective-permute-start(f32[30,512]{1,0:T(8,128)S(1)} %slice.257), channel_id=1, source_target_pairs={{4,0},{8,4},{12,8},{16,12},{20,16},{24,20},{28,24},{5,1},{9,5},{13... | collective-permute-start | bytes 184328 | tf_op jit(solution)/shard_map/ppermute | solution.py:10
  (19 other events, 84.2 us)
Sparse Core Ops, SparseCore 0:
  33.8 21.5 all-gather.4
  57.0 22.5 all-gather.2
  88.7 51.3 all-reduce.2
  198.1 66.5 reduce-scatter.1
where the time goes:
time: 274 us; the launch traced here: 273 us
  waiting for transfers between devices  163 us (59%)
  blocking collectives  45.5 us (17%)
  matrix products  33.1 us (12%)
  between operations  14.5 us (5%)
  starting transfers between devices  6.96 us (3%)
  other arithmetic  6.52 us (2%)
  local copies, waits for them, and re-layouts  3.94 us (1%)
    psum x1, waiting for transfers between devices, shards(): summed = lax.psum(partial_value.astype(jnp.bfloat16), 'tp')  51.5 us
    all_to_all x1, waiting for transfers between devices, shards(): lax.all_to_all(summed.reshape(experts, capacity, model_width), 'sp', spli...  47.7 us
    reduce_scatter x1, waiting for transfers between devices, shards(): lax.psum_scatter(lax.dot_general(mixer_grad, act_conv, contract_first, pr...  40.9 us
    all_to_all x1, blocking collectives, shards(): lax.all_to_all(sent_rows, 'sp', split_axis=0, concat_axis=0, tiled=True)  21.7 us
    all_gather x1, waiting for transfers between devices, shards(): lax.all_gather(shared_rows[1], 'tp', axis=1, tiled=True)  17.9 us
    all_to_all x1, blocking collectives, shards(): lax.all_to_all(sent_grad, 'sp', split_axis=0, concat_axis=0, tiled=True)  17.6 us
    psum x1, blocking collectives, shards(): lax.psum((jnp.sum(norm_output_gradient, axis=1), jnp.sum(norm_output_grad...  6.16 us
    all_to_all x1, starting transfers between devices, shards(): lax.all_to_all(summed.reshape(experts, capacity, model_width), 'sp', spli...  5.51 us
  transfers between devices with their start and end apart: 6, of which 6 were waited for; matrix products, arithmetic and copies ran while one was open for 9% of the time, Pallas kernels for 0%

commit v1 on v0

--- a/solution.py
+++ b/solution.py
@@ -2,6 +2,11 @@
 import jax.numpy as jnp
 from jax import lax
 from jax.sharding import PartitionSpec as P
+
+
+def summed_here(block, axis):
+    pieces = lax.all_gather(block, axis)
+    return jnp.sum(pieces, axis=0)
 
 
 def from_behind(value, axis, steps):
@@ -102,7 +107,7 @@
     partial_value = lax.dot_general(
         grad_gpre, w_first, contract_last, preferred_element_type=jnp.float32
     ) + lax.dot_general(grad_upre, w_third, contract_last, preferred_element_type=jnp.float32)
-    summed = lax.psum(partial_value.astype(jnp.bfloat16), "tp")
+    summed = summed_here(partial_value.astype(jnp.bfloat16), "tp")
     home_rows = lax.all_to_all(
         summed.reshape(experts, capacity, model_width),
         "sp",

time: 274 us -> 289 us (1.055)
  other arithmetic: 6.52 us -> 13.7 us
  waiting for transfers between devices: 163 us -> 170 us
    all_gather x0 -> x1, waiting for transfers between devices: none -> 58.4 us  [summed_here(): pieces = lax.all_gather(block, axis)]
    psum x1 -> x0, waiting for transfers between devices: 51.5 us -> none  [shards(): summed = lax.psum(partial_value.astype(jnp.bfloat16), 'tp')]
    reduce_sum x0 -> x1, other arithmetic: none -> 7.2 us  [summed_here(): return jnp.sum(pieces, axis=0)]
  transfers between devices with their start and end apart: 6 -> 6, of which waited for: 6 -> 6; matrix products, arithmetic and copies ran while one was open for 9% -> 8% of each run, Pallas kernels for 0% -> 0%
where the time goes in v1:
time: 289 us; the launch traced here: 288 us
  waiting for transfers between devices  170 us (59%)
  blocking collectives  45.5 us (16%)
  matrix products  33.1 us (11%)
  between operations  14.5 us (5%)
  other arithmetic  13.7 us (5%)
  starting transfers between devices  7.15 us (2%)
  local copies, waits for them, and re-layouts  3.93 us (1%)
    all_gather x1, waiting for transfers between devices, summed_here(): pieces = lax.all_gather(block, axis)  58.4 us
    all_to_all x1, waiting for transfers between devices, shards(): lax.all_to_all(summed.reshape(experts, capacity, model_width), 'sp', spli...  48.2 us
    reduce_scatter x1, waiting for transfers between devices, shards(): lax.psum_scatter(lax.dot_general(mixer_grad, act_conv, contract_first, pr...  41.3 us
    all_to_all x1, blocking collectives, shards(): lax.all_to_all(sent_rows, 'sp', split_axis=0, concat_axis=0, tiled=True)  21.7 us
    all_gather x1, waiting for transfers between devices, shards(): lax.all_gather(shared_rows[1], 'tp', axis=1, tiled=True)  17.9 us
    all_to_all x1, blocking collectives, shards(): lax.all_to_all(sent_grad, 'sp', split_axis=0, concat_axis=0, tiled=True)  17.6 us
    reduce_sum x1, other arithmetic, summed_here(): return jnp.sum(pieces, axis=0)  7.2 us
    psum x1, blocking collectives, shards(): lax.psum((jnp.sum(norm_output_gradient, axis=1), jnp.sum(norm_output_grad...  6.18 us
  transfers between devices with their start and end apart: 6, of which 6 were waited for; matrix products, arithmetic and copies ran while one was open for 8% of the time, Pallas kernels for 0%

profile of v1, /device:TPU:0, one launch (start us, length us, event | category | flops | bytes accessed | tf_op | source)
XLA Modules:
  0.0 288.0 jit_solution(13804271145828696299)
XLA Ops:
  7.3 0.9 copy.31
  9.8 0.7 multiply_add_fusion
  10.6 1.3 convolution_convert_fusion.4
  11.9 21.7 %all_to_all.15 = bf16[8,16,2048]{2,1,0:T(8,128)(2,1)} all-to-all(bf16[8,16,2048]{2,1,0:T(8,128)(2,1)S(1)} %bitcast.89), channel_id=1, replica_groups=mesh['sp'=8,'tp'=4] {'sp'}, dimensions={0} | all-to-all | bytes 1048576 | tf_op jit(solution)/shard_map/all_to_all | solution.py:69
  34.2 17.6 %all_to_all.16 = bf16[8,16,2048]{2,1,0:T(8,128)(2,1)} all-to-all(bf16[8,16,2048]{2,1,0:T(8,128)(2,1)S(1)} %bitcast.88), channel_id=1, replica_groups=mesh['sp'=8,'tp'=4] {'sp'}, dimensions={0} | all-to-all | bytes 1048576 | tf_op jit(solution)/shard_map/all_to_all | solution.py:70
  51.9 3.5 %all-gather.7.cloned.1.call-done = bf16[8,64,2048]{2,1,0:T(8,128)(2,1)} async-done(((bf16[8,16,2048]{2,1,0:T(8,128)(2,1)}), bf16[8,64,2048]{2,1,0:T(8,128)(2,1)}) %all-gather.7.cloned.1.call-update) | async-done | bytes 2097168 | tf_op jit(solution)/shard_map/all_gather | solution.py:73
  55.4 4.0 %fusion.7 = f32[512,512]{1,0:T(8,128)} fusion(bf16[512,2048]{1,0:T(8,128)(2,1)} %bitcast.121, bf16[1,2048,512]{2,1,0:T(8,128)(2,1)S(1)} %copy-done), kind=kOutput, calls=%fused_computation.44 | convolution fusion | flops 1073741824 | bytes 5242880 | tf_op jit(solution)/shard_map/dot_general | solution.py:86
  59.4 2.3 fusion.10
  61.7 17.9 %all-gather.5.cloned.1.call-done = bf16[8,64,2048]{2,1,0:T(8,128)(2,1)} async-done(((bf16[8,16,2048]{2,1,0:T(8,128)(2,1)}), bf16[8,64,2048]{2,1,0:T(8,128)(2,1)}) %all-gather.5.cloned.1.call-update) | async-done | bytes 2097168 | tf_op jit(solution)/shard_map/all_gather | solution.py:74
  79.6 4.4 %multiply_convert_fusion.1 = (bf16[512,512]{1,0:T(8,128)(2,1)S(1)}, bf16[512,512]{1,0:T(8,128)(2,1)S(1)}) fusion(f32[512,512]{1,0:T(8,128)} %fusion.7, f32[512,512]{1,0:T(8,128)} %fusion.10, bf16[512,2048]{1,0:T(8,128)(2,1)} %bitcast.125, bf16[1,512,2048]{2,1,0:T(8,128)(2,1)} %param.23), kind=kOutput, calls=%fused_computation.55 | convolution fusion | flops 1077149696 | bytes 7340032 | tf_op jit(solution)/shard_map/dot_general | solution.py:94
  84.0 1.3 fusion.5
  85.3 0.6 copy-done.2
  85.9 2.6 add_convert_fusion
  88.6 58.4 %all-gather.9.cloned.1.call-done = bf16[2048,2048]{1,0:T(8,128)(2,1)} async-done(((bf16[512,2048]{1,0:T(8,128)(2,1)}), bf16[2048,2048]{1,0:T(8,128)(2,1)}) %all-gather.9.cloned.1.call-update) | async-done | bytes 8388624 | tf_op jit(solution)/shard_map/all_gather | solution.py:8
  147.0 7.2 %reduce_sum.54 = bf16[512,2048]{1,0:T(8,128)(2,1)} reduce(bf16[4,512,2048]{2,1,0:T(8,128)(2,1)} %bitcast.86, bf16[]{:T(256)} %constant.27.clone.1), dimensions={0}, to_apply=%region_6.7 | reduce | flops 3145728 | bytes 10485762 | tf_op jit(solution)/shard_map/reduce_sum | solution.py:9
  154.2 5.5 %all-to-all-start.2 = ((bf16[8,64,2048]{2,1,0:T(8,128)(2,1)}), bf16[8,64,2048]{2,1,0:T(8,128)(2,1)}, u32[]{:S(2)}, u32[]{:S(2)}) async-start(bf16[8,64,2048]{2,1,0:T(8,128)(2,1)} %bitcast.87), calls=%async_computation.2 | async-start | bytes 4194304 | tf_op jit(solution)/shard_map/all_to_all | solution.py:111
  160.3 48.2 %all-to-all-done.2 = bf16[8,64,2048]{2,1,0:T(8,128)(2,1)} async-done(((bf16[8,64,2048]{2,1,0:T(8,128)(2,1)}), bf16[8,64,2048]{2,1,0:T(8,128)(2,1)}, u32[]{:S(2)}, u32[]{:S(2)}) %all-to-all-start.2) | async-done | bytes 2097184 | tf_op jit(solution)/shard_map/all_to_all | solution.py:111
  208.5 2.1 fusion.4
  210.6 2.1 convolution_convert_fusion
  212.7 0.6 fusion.130
  213.3 0.7 fusion.129
  214.1 4.4 %fusion.1 = bf16[1,2048,512]{2,1,0:T(8,128)(2,1)} fusion(bf16[512,2048]{1,0:T(8,128)(2,1)} %bitcast.122, bf16[512,512]{1,0:T(8,128)(2,1)S(1)} %copy-done.7), kind=kOutput, calls=%fused_computation.35 | convolution fusion | flops 1074790400 | bytes 4718592 | tf_op jit(solution)/shard_map/dot_general | solution.py:104
  218.5 2.7 fusion.2
  221.2 1.5 fusion.128
  222.7 6.2 %all-reduce = (f32[128]{0:T(128)S(1)}, f32[128]{0:T(128)S(1)}) all-reduce(f32[128]{0:T(128)} %get-tuple-element.6, f32[128]{0:T(128)} %get-tuple-element.5), channel_id=1, replica_groups=mesh['sp'=8,'tp'=4] {'tp'}, use_global_device_ids=true, to_apply=%region_10.11 | all-reduce | flops 256 | bytes 2048 | tf_op jit(solution)/shard_map/psum | solution.py:146
  228.9 0.8 fusion.27
  229.9 1.3 collective-permute-start
  231.2 4.3 %fusion = bf16[1,2048,512]{2,1,0:T(8,128)(2,1)} fusion(bf16[512,2048]{1,0:T(8,128)(2,1)} %bitcast.123, bf16[512,512]{1,0:T(8,128)(2,1)S(1)} %copy-done.5), kind=kOutput, calls=%fused_computation.34 | convolution fusion | flops 1074790400 | bytes 4718592 | tf_op jit(solution)/shard_map/dot_general | solution.py:101
  235.5 0.7 collective-permute-done
  236.4 2.0 fusion.32
  238.4 41.3 %reduce-scatter.2.cloned.1.call-done = bf16[256,512]{1,0:T(8,128)(2,1)} async-done(((bf16[2048,512]{1,0:T(8,128)(2,1)}), bf16[256,512]{1,0:T(8,128)(2,1)}) %reduce-scatter.2.cloned.1.call-update) | async-done | bytes 262160 | tf_op jit(solution)/shard_map/reduce_scatter | solution.py:129
  279.7 1.8 convert_element_type.74
  (119 shorter events, 3.0 us)
Async XLA Ops:
  7.2 48.3 %copy-start = (bf16[1,2048,512]{2,1,0:T(8,128)(2,1)S(1)}, bf16[1,2048,512]{2,1,0:T(8,128)(2,1)}, u32[]{:S(2)}) copy-start(bf16[1,2048,512]{2,1,0:T(8,128)(2,1)} %param.21) | copy-start | bytes 6291460
  7.2 26.5 %copy-start.39 = (f32[128,2]{0,1:T(2,128)S(1)}, f32[128,2]{0,1:T(2,128)}, u32[]{:S(2)}) copy-start(f32[128,2]{0,1:T(2,128)} %param.15) | copy-start | bytes 3076
  7.2 26.7 %copy-start.3 = (bf16[128,2048]{1,0:T(8,128)(2,1)S(1)}, bf16[128,2048]{1,0:T(8,128)(2,1)}, u32[]{:S(2)}) copy-start(bf16[128,2048]{1,0:T(8,128)(2,1)} %param.12) | copy-start | bytes 1572868
  7.2 48.2 %all-gather.7.cloned.1.call-start = ((), (), s32[]{:S(2)}) async-start(), calls=%async_computation.5 | async-start | bytes 2621440 | tf_op jit(solution)/shard_map/all_gather | solution.py:73
  33.7 45.9 %all-gather.5.cloned.1.call-start = ((), (), s32[]{:S(2)}) async-start(), calls=%async_computation.4 | async-start | bytes 2621440 | tf_op jit(solution)/shard_map/all_gather | solution.py:74
  51.9 95.1 %all-gather.9.cloned.1.call-start = ((), (), s32[]{:S(2)}) async-start(), calls=%async_computation.7 | async-start | bytes 10485760 | tf_op jit(solution)/shard_map/all_gather | solution.py:8
  154.2 54.3 %all-to-all-start.2 = ((bf16[8,64,2048]{2,1,0:T(8,128)(2,1)}), bf16[8,64,2048]{2,1,0:T(8,128)(2,1)}, u32[]{:S(2)}, u32[]{:S(2)}) async-start(bf16[8,64,2048]{2,1,0:T(8,128)(2,1)} %bitcast.87), calls=%async_computation.2 | async-start | bytes 4194304 | tf_op jit(solution)/shard_map/all_to_all | solution.py:111
  159.7 50.8 %copy-start.8 = (bf16[128,512]{1,0:T(8,128)(2,1)S(1)}, bf16[128,512]{1,0:T(8,128)(2,1)}, u32[]{:S(2)}) copy-start(bf16[128,512]{1,0:T(8,128)(2,1)} %param.16) | copy-start | bytes 393220
  159.7 50.8 %copy-start.37 = (f32[512]{0:T(512)S(1)}, f32[512]{0:T(512)}, u32[]{:S(2)}) copy-start(f32[512]{0:T(512)} %param.18) | copy-start | bytes 6148
  159.7 120.0 %reduce-scatter.2.cloned.1.call-start = ((), (), s32[]{:S(2)}) async-start(), calls=%async_computation.6 | async-start | bytes 2359296 | tf_op jit(solution)/shard_map/reduce_scatter | solution.py:129
  221.2 10.1 %copy-start.5 = (bf16[512,512]{1,0:T(8,128)(2,1)S(1)}, bf16[512,512]{1,0:T(8,128)(2,1)}, u32[]{:S(2)}) copy-start(bf16[512,512]{1,0:T(8,128)(2,1)} %copy-done.4) | copy-start | bytes 1572868
  229.7 6.5 %copy-start.10 = (f32[1,512]{1,0:T(1,128)S(1)}, f32[1,512]{1,0:T(1,128)}, u32[]{:S(2)}) copy-start(f32[1,512]{1,0:T(1,128)} %get-tuple-element.34) | copy-start | bytes 6148
  229.7 6.5 %copy-start.11 = (f32[1,512]{1,0:T(1,128)S(1)}, f32[1,512]{1,0:T(1,128)}, u32[]{:S(2)}) copy-start(f32[1,512]{1,0:T(1,128)} %get-tuple-element.35) | copy-start | bytes 6148
  229.7 6.5 %copy-start.12 = (f32[1,512]{1,0:T(1,128)S(1)}, f32[1,512]{1,0:T(1,128)}, u32[]{:S(2)}) copy-start(f32[1,512]{1,0:T(1,128)} %get-tuple-element.36) | copy-start | bytes 6148
  229.7 6.5 %copy-start.13 = (f32[1,512]{1,0:T(1,128)S(1)}, f32[1,512]{1,0:T(1,128)}, u32[]{:S(2)}) copy-start(f32[1,512]{1,0:T(1,128)} %get-tuple-element.37) | copy-start | bytes 6148
  229.7 6.5 %copy-start.14 = (f32[1,512]{1,0:T(1,128)S(1)}, f32[1,512]{1,0:T(1,128)}, u32[]{:S(2)}) copy-start(f32[1,512]{1,0:T(1,128)} %get-tuple-element.38) | copy-start | bytes 6148
  229.7 6.5 %copy-start.15 = (f32[1,512]{1,0:T(1,128)S(1)}, f32[1,512]{1,0:T(1,128)}, u32[]{:S(2)}) copy-start(f32[1,512]{1,0:T(1,128)} %get-tuple-element.39) | copy-start | bytes 6148
  229.7 6.5 %copy-start.16 = (f32[1,512]{1,0:T(1,128)S(1)}, f32[1,512]{1,0:T(1,128)}, u32[]{:S(2)}) copy-start(f32[1,512]{1,0:T(1,128)} %get-tuple-element.40) | copy-start | bytes 6148
  229.7 6.5 %copy-start.17 = (f32[1,512]{1,0:T(1,128)S(1)}, f32[1,512]{1,0:T(1,128)}, u32[]{:S(2)}) copy-start(f32[1,512]{1,0:T(1,128)} %get-tuple-element.41) | copy-start | bytes 6148
  229.7 6.5 %copy-start.18 = (f32[1,512]{1,0:T(1,128)S(1)}, f32[1,512]{1,0:T(1,128)}, u32[]{:S(2)}) copy-start(f32[1,512]{1,0:T(1,128)} %get-tuple-element.11) | copy-start | bytes 6148
  229.8 6.5 %copy-start.19 = (f32[1,512]{1,0:T(1,128)S(1)}, f32[1,512]{1,0:T(1,128)}, u32[]{:S(2)}) copy-start(f32[1,512]{1,0:T(1,128)} %get-tuple-element.12) | copy-start | bytes 6148
  229.8 6.5 %copy-start.20 = (f32[1,512]{1,0:T(1,128)S(1)}, f32[1,512]{1,0:T(1,128)}, u32[]{:S(2)}) copy-start(f32[1,512]{1,0:T(1,128)} %get-tuple-element.13) | copy-start | bytes 6148
  229.8 6.5 %copy-start.21 = (f32[1,512]{1,0:T(1,128)S(1)}, f32[1,512]{1,0:T(1,128)}, u32[]{:S(2)}) copy-start(f32[1,512]{1,0:T(1,128)} %get-tuple-element.14) | copy-start | bytes 6148
  229.8 6.5 %copy-start.22 = (f32[1,512]{1,0:T(1,128)S(1)}, f32[1,512]{1,0:T(1,128)}, u32[]{:S(2)}) copy-start(f32[1,512]{1,0:T(1,128)} %get-tuple-element.15) | copy-start | bytes 6148
  229.8 6.5 %copy-start.23 = (f32[1,512]{1,0:T(1,128)S(1)}, f32[1,512]{1,0:T(1,128)}, u32[]{:S(2)}) copy-start(f32[1,512]{1,0:T(1,128)} %get-tuple-element.16) | copy-start | bytes 6148
  229.8 6.5 %copy-start.24 = (f32[1,512]{1,0:T(1,128)S(1)}, f32[1,512]{1,0:T(1,128)}, u32[]{:S(2)}) copy-start(f32[1,512]{1,0:T(1,128)} %get-tuple-element.17) | copy-start | bytes 6148
  229.8 6.5 %copy-start.25 = (f32[1,512]{1,0:T(1,128)S(1)}, f32[1,512]{1,0:T(1,128)}, u32[]{:S(2)}) copy-start(f32[1,512]{1,0:T(1,128)} %get-tuple-element.18) | copy-start | bytes 6148
  229.8 6.5 %copy-start.26 = (f32[1,512]{1,0:T(1,128)S(1)}, f32[1,512]{1,0:T(1,128)}, u32[]{:S(2)}) copy-start(f32[1,512]{1,0:T(1,128)} %get-tuple-element.19) | copy-start | bytes 6148
  229.8 6.5 %copy-start.27 = (f32[1,512]{1,0:T(1,128)S(1)}, f32[1,512]{1,0:T(1,128)}, u32[]{:S(2)}) copy-start(f32[1,512]{1,0:T(1,128)} %get-tuple-element.20) | copy-start | bytes 6148
  229.8 6.5 %copy-start.28 = (f32[1,512]{1,0:T(1,128)S(1)}, f32[1,512]{1,0:T(1,128)}, u32[]{:S(2)}) copy-start(f32[1,512]{1,0:T(1,128)} %get-tuple-element.21) | copy-start | bytes 6148
  229.8 6.5 %copy-start.29 = (f32[1,512]{1,0:T(1,128)S(1)}, f32[1,512]{1,0:T(1,128)}, u32[]{:S(2)}) copy-start(f32[1,512]{1,0:T(1,128)} %get-tuple-element.22) | copy-start | bytes 6148
  229.9 6.2 %collective-permute-start = (f32[30,512]{1,0:T(8,128)S(1)}, f32[30,512]{1,0:T(8,128)S(1)}, u32[]{:S(2)}, u32[]{:S(2)}) collective-permute-start(f32[30,512]{1,0:T(8,128)S(1)} %slice.257), channel_id=1, source_target_pairs={{4,0},{8,4},{12,8},{16,12},{20,16},{24,20},{28,24},{5,1},{9,5},{13... | collective-permute-start | bytes 184328 | tf_op jit(solution)/shard_map/ppermute | solution.py:15
  (19 other events, 82.3 us)
Sparse Core Ops, SparseCore 0:
  33.8 21.5 all-gather.6
  57.0 22.5 all-gather.4
  88.7 58.2 all-gather.8
  212.8 66.7 reduce-scatter.1
